TPU v7x, 512 devices: a whole 4x8x8 slice. The times are simulated.
512 devices in a mesh: sp: 32 (over z, x), dp: 16 (over y, core).
Axes of the slice: x: 4, y: 8, z: 8, core: 2. Of those that a mesh axis runs over, the one named last changes fastest.
Arguments:
- query_rows: bfloat16 [16, 4096, 2048], P('dp', 'sp'), may hold values from -6 to 6
- key_rows: bfloat16 [16, 4096, 2048], P('dp', 'sp'), may hold values from -6 to 6
- value_rows: bfloat16 [16, 4096, 2048], P('dp', 'sp'), may hold values from -6 to 6
- decay_low: bfloat16 [16, 4096, 128], P('dp', 'sp'), may hold values from -5 to 5
- rate_low: bfloat16 [16, 4096, 128], P('dp', 'sp'), may hold values from -4 to 4
- decay_up: bfloat16 [128, 2048], replicated, may hold values from -0.5 to 0.5
- rate_up: bfloat16 [128, 2048], replicated, may hold values from -0.5 to 0.5
- decay_base: float32 [2048], replicated, may hold values from -12 to -2
- norm_gain: float32 [2048], replicated, may hold values from 0.1 to 1.9
- out_weight: bfloat16 [2048, 2048], P(None, 'dp'), may hold values from -0.125 to 0.125
Outputs:
- layer_out: bfloat16 [16, 4096, 2048], P('dp', 'sp')
All inputs are finite; a program needn't handle non-finite values.
Results may differ from a plain program's by a relative error of at most 0.005.
Values may be sent and summed in bfloat16 or wider, within the bound.
A program may use at most 128 MiB of HBM per device.

v0:
```python
import jax
import jax.numpy as jnp
from jax import lax
from jax.experimental import pallas as pl
from jax.experimental.pallas import tpu as pltpu
from jax.sharding import PartitionSpec as P

F32 = jnp.float32
BF16 = jnp.bfloat16
C = 128
PAIRS = 16
SP = 32
DPN = 16
YN = 8
MSG = 80
DECAY_SCALE = 0.6065306597126334
MESH = pl.DeviceIdType.MESH


def split(x):
    high = x.astype(BF16)
    return high, (x - high.astype(F32)).astype(BF16)


def nn(a, b):
    return jnp.dot(a, b, preferred_element_type=F32)


def nt(a, b):
    return lax.dot_general(a, b, (((1,), (1,)), ((), ())), preferred_element_type=F32)


def rows_of(*parts):
    return jnp.concatenate(parts, axis=0)


def lanes_of(*parts):
    return jnp.concatenate(parts, axis=1)


def sigmoid(x):
    return 1.0 / (1.0 + jnp.exp(-x))


def iotas():
    return (
        lax.broadcasted_iota(jnp.int32, (C, C), 0),
        lax.broadcasted_iota(jnp.int32, (C, C), 1),
    )


def roll_half(x):
    return pltpu.roll(x, 64, 1)


def pair_front(pair, q_ref, k_ref, v_ref, sq_ref, rl_ref, du_ref, ru_ref, base_ref):
    row, col = iotas()
    first = col < 64
    at = pl.ds(pl.multiple_of(pair * C, C), C)
    decay_pre = (base_ref[pl.ds(pair, 1), :] + nn(sq_ref[...], du_ref[:, at])).astype(BF16).astype(F32)
    rate_pre = nn(rl_ref[...], ru_ref[:, at]).astype(BF16).astype(F32)
    log_decay = -DECAY_SCALE * sigmoid(decay_pre)
    rate = sigmoid(rate_pre)
    tri = jnp.where(row >= col, 1.0, 0.0).astype(BF16)
    ld_h, ld_l = split(log_decay)
    running = nn(lanes_of(tri, tri), rows_of(ld_h, ld_l))
    key = k_ref[:, at].astype(F32)
    query = q_ref[:, at].astype(F32)
    same = jnp.where((row < 64) == first, 1.0, 0.0).astype(BF16)
    sq_h, sq_l = split(key * key)
    unit = key * lax.rsqrt(1.0 + nn(lanes_of(sq_h, sq_l), rows_of(same, same)))
    erase = unit * rate
    centre = running[63:64, :]
    final = running[C - 1 : C, :]
    up = jnp.exp(running - centre)
    down = jnp.exp(centre - running)
    before = jnp.exp(running - log_decay - centre)
    from_start = jnp.exp(centre)
    to_end = jnp.exp(final - centre)
    f1 = unit * before
    f2 = query * up
    g1 = key * down
    g2 = erase * down
    return f1, f2, g1, g2, f1 * from_start, f2 * from_start, g1 * to_end, g2 * to_end, jnp.exp(final)


def pair_body(pair, refs, msg_ref, p_ref, o_ref):
    q_ref, k_ref, v_ref, sq_ref, rl_ref, du_ref, ru_ref, base_ref = refs
    row, col = iotas()
    first = col < 64
    first_b = lax.broadcasted_iota(jnp.int32, (2 * C, C), 1) < 64
    strict = row > col
    within = row >= col
    at = pl.ds(pl.multiple_of(pair * C, C), C)
    f1, f2, g1, g2, es, qs, ke, ee, efin = pair_front(pair, *refs)
    f_h, f_l = split(rows_of(f1, f2))
    zero2 = jnp.zeros((2 * C, C), BF16)
    fa_h, fa_l = jnp.where(first_b, f_h, zero2), jnp.where(first_b, f_l, zero2)
    fb_h, fb_l = jnp.where(first_b, zero2, f_h), jnp.where(first_b, zero2, f_l)
    g_h, g_l = split(rows_of(g1, g2))
    gg = lanes_of(g_h, g_h)
    grams = [
        nt(lanes_of(fa_h, fa_l), gg) + nt(fa_h, g_l),
        nt(lanes_of(fb_h, fb_l), gg) + nt(fb_h, g_l),
    ]
    v_roll = roll_half(v_ref[:, at].astype(F32)).astype(BF16)
    zero1 = jnp.zeros((C, C), BF16)
    eye = jnp.where(row == col, 1.0, 0.0)
    ep, kp, rk, re, x = [], [], [], [], []
    differ = row ^ col
    for g in grams:
        kp.append(split(jnp.where(strict, g[:C, :C], 0.0)))
        ep.append(split(jnp.where(strict, g[:C, C:], 0.0)))
        rk.append(split(jnp.where(within, g[C:, :C], 0.0)))
        re.append(split(jnp.where(within, g[C:, C:], 0.0)))
        x.append(eye - jnp.where(differ == 1, ep[-1][0].astype(F32), 0.0))
    size = 2
    while size < C:
        level = (differ >= size) & (differ < 2 * size)
        xb = [a.astype(BF16) for a in x]
        mid = [nn(xb[i], jnp.where(level, ep[i][0], zero1)).astype(BF16) for i in range(2)]
        x = [x[i] - nn(mid[i], xb[i]) for i in range(2)]
        size *= 2
    ee_t = split(ee.T)
    ke_t = split(ke.T)
    outs = []
    for i in range(2):
        mine = first if i == 0 else ~first
        xb = x[i].astype(BF16)
        carried = nn(lanes_of(*kp[i]), rows_of(v_roll, v_roll))
        rhs = jnp.where(mine, es, carried)
        s0 = nn(xb, rhs.astype(BF16)).astype(BF16)
        resid = rhs - s0.astype(F32) - nn(lanes_of(*ep[i]), rows_of(s0, s0))
        sol = s0.astype(F32) + nn(xb, resid.astype(BF16))
        n_h, n_l = split(-sol)
        v_mine = jnp.where(mine, zero1, v_roll)
        w_h = rows_of(n_h, v_mine)
        half = slice(64 * i, 64 * i + 64)
        l_h = rows_of(lanes_of(ee_t[0][half], ke_t[0][half]), lanes_of(re[i][0], rk[i][0]))
        l_l = rows_of(lanes_of(ee_t[1][half], ke_t[1][half]), lanes_of(re[i][1], rk[i][1]))
        outs.append(nn(l_h, w_h) + nn(l_l, w_h) + nn(rows_of(ee_t[0][half], re[i][0]), n_l))
    d_h, d_l = split(jnp.broadcast_to(efin, (16, C)))
    low_rows = lax.broadcasted_iota(jnp.int32, (16, C), 0) < 8
    d_tile = jnp.where(low_rows, d_h, d_l)
    for i in range(2):
        msg_ref[2 * pair + i, pl.ds(0, 64), :] = outs[i][:64].astype(BF16)
        msg_ref[2 * pair + i, pl.ds(64, 16), :] = d_tile
    p_all = qs + jnp.where(first, outs[0][64:], outs[1][64:])
    o_all = roll_half(jnp.where(first, outs[1][64:], outs[0][64:]))
    p_h, p_l = split(p_all)
    p_ref[pair] = lanes_of(p_h, p_l)
    o_ref[pair] = o_all


def compose_chunks(odd, msg_ref, zs_ref, g_ref):
    row = lax.broadcasted_iota(jnp.int32, (64, C), 0)
    col = lax.broadcasted_iota(jnp.int32, (64, C), 1)
    left = col < 64
    groups, per = 4, 8
    state = [jnp.where(row == col, 1.0, 0.0) for _ in range(groups)]
    zero = jnp.zeros((64, C), BF16)
    for step in range(per):
        for g in range(groups):
            c = g * per + step
            g_ref[g, pl.ds(64 * step, 64), :] = state[g]
            m = msg_ref[c, pl.ds(0, 64), :].astype(F32)
            tile = msg_ref[c, pl.ds(64, 16), :].astype(F32)
            d = tile[0:1, :] + tile[8:9, :]
            m = jnp.where(odd, roll_half(m), m)
            d = jnp.where(odd, roll_half(jnp.broadcast_to(d, (8, C)))[0:1, :], d)
            trans = jnp.where(left, m + jnp.where(row == col, d, 0.0), 0.0)
            add = jnp.where(left, 0.0, m)
            t_h, t_l = split(trans)
            lhs = lanes_of(jnp.where(left, t_h.astype(F32), roll_half(t_l.astype(F32))).astype(BF16), t_h)
            s_h, s_l = split(state[g])
            state[g] = nn(lhs, rows_of(s_h, s_h, s_l, zero)) + add
    starts = [None]
    z = jnp.where(left, roll_half(state[0]), 0.0)
    for g in range(1, groups):
        starts.append(z)
        if g < groups - 1:
            z = jnp.where(left, apply_state(state[g], z, left) + roll_half(state[g]), 0.0)
    for g in range(groups):
        stack = g_ref[g]
        wide = lax.broadcasted_iota(jnp.int32, (64 * per, C), 1) < 64
        total = roll_half(stack)
        if g > 0:
            total = total + apply_state(stack, starts[g], wide)
        for step in range(per):
            zc = total[64 * step : 64 * step + 64]
            packed = jnp.where(left[:32], zc[:32], roll_half(zc[32:]))
            zs_ref[g * per + step] = packed.astype(BF16)


def apply_state(stack, z, left):
    t_h, t_l = split(jnp.where(left, stack, 0.0))
    z_h, z_l = split(z)
    zero = jnp.zeros((64, C), BF16)
    lhs = lanes_of(jnp.where(left, t_h.astype(F32), roll_half(t_l.astype(F32))).astype(BF16), t_h)
    return nn(lhs, rows_of(z_h, z_h, z_l, zero))


def pair_finish(pair, z_ref, p_ref, o_ref, gain_ref, mix_ref):
    row, col = iotas()
    left = lax.broadcasted_iota(jnp.int32, (32, C), 1) < 64
    za = z_ref[2 * pair].astype(F32)
    zb = z_ref[2 * pair + 1].astype(F32)
    zw = rows_of(
        jnp.where(left, za, 0.0),
        jnp.where(left, roll_half(za), 0.0),
        jnp.where(left, 0.0, roll_half(zb)),
        jnp.where(left, 0.0, zb),
    ).astype(BF16)
    read = o_ref[pair] + nn(p_ref[pair], rows_of(zw, zw))
    mean_w = jnp.where((row < 64) == (col < 64), 1.0 / 64, 0.0).astype(BF16)
    mean_w = rows_of(mean_w, mean_w)
    centred = read - nn(lanes_of(*split(read)), mean_w)
    var = nn(lanes_of(*split(centred * centred)), mean_w)
    at = pl.ds(pl.multiple_of(pair * C, C), C)
    mix_ref[:, at] = (centred * lax.rsqrt(var + 1.0) * gain_ref[pl.ds(pair, 1), :]).astype(BF16)


def project(mix_ref, w_ref, out_ref):
    @pl.loop(0, YN)
    def _(y):
        acc = jnp.zeros((C, 2 * C), F32)
        for k in range(8):
            w = lanes_of(w_ref[2 * y, pl.ds(256 * k, 256), :], w_ref[2 * y + 1, pl.ds(256 * k, 256), :])
            acc = acc + nn(mix_ref[:, pl.ds(256 * k, 256)], w)
        out_ref[:, pl.ds(pl.multiple_of(y * 256, 256), 256)] = acc.astype(BF16)


def remote(src, dst, send, recv, **where):
    return pltpu.make_async_remote_copy(
        src_ref=src, dst_ref=dst, send_sem=send, recv_sem=recv, device_id=where, device_id_type=MESH
    )


def kernel(
    q_ref,
    k_ref,
    v_ref,
    dl_ref,
    rl_ref,
    du_ref,
    ru_ref,
    base_ref,
    gain_ref,
    w_ref,
    out_ref,
    sq_ref,
    msg_ref,
    got_ref,
    group_ref,
    zs_ref,
    zgot_ref,
    p_ref,
    o_ref,
    mix_ref,
    wall_ref,
    own_sem,
    msg_send,
    msg_recv,
    z_send,
    z_recv,
    ring_send,
    ring_recv,
    side_send,
    side_recv,
):
    me = lax.axis_index("sp")
    dp = lax.axis_index("dp")
    core = lax.rem(dp, 2)
    chip = lax.div(dp, 2)
    partner = dp + 1 - 2 * core
    up = lax.rem(dp + 2, DPN)
    down = lax.rem(dp + DPN - 2, DPN)

    barrier = pltpu.get_barrier_semaphore()

    @pl.loop(1, SP)
    def _(j):
        pl.semaphore_signal(
            barrier, inc=1, device_id={"sp": lax.rem(me + j, SP)}, device_id_type=MESH
        )

    for other in (partner, up, down):
        pl.semaphore_signal(barrier, inc=1, device_id={"dp": other}, device_id_type=MESH)
    own = pltpu.make_async_copy(w_ref, wall_ref.at[dp], own_sem)
    own.start()
    sq_ref[...] = jnp.tanh(dl_ref[...].astype(F32)).astype(BF16)
    own.wait()
    pl.semaphore_wait(barrier, SP + 2)

    def piece(column, half):
        return wall_ref.at[column, pl.ds(half * 1024, 1024), :]

    def ring(way, order, column, half):
        ref = piece(column, half)
        return remote(ref, ref, ring_send.at[way, order], ring_recv.at[way, order], dp=(up, down)[way])

    def side(slot, column, half):
        ref = piece(column, half)
        return remote(ref, ref, side_send.at[slot], side_recv.at[slot], dp=partner)

    for order in range(2):
        ring(0, order, dp, order).start()
        ring(1, order, dp, 1 - order).start()
        side(14 + order, dp, order).start()

    def ring_step(s):
        near = lax.div(s, 2) + 1
        half0 = lax.rem(s, 2)
        for way in range(2):
            half = half0 if way == 0 else 1 - half0
            column = lax.rem(chip + (YN - near if way == 0 else near), YN) * 2 + core
            ring(way, s, column, half).wait_recv()

            @pl.when(s < 5)
            def _():
                ring(way, s + 2, column, half).start()

            side(2 * s + way, column, half).start()

    def send_message(head):
        return remote(
            msg_ref.at[head], got_ref.at[me], msg_send.at[head], msg_recv.at[me], sp=head
        )

    def send_pair(pair):
        for i in range(2):
            head = 2 * pair + i

            @pl.when(head != me)
            def _():
                send_message(head).start()

    first_pair = lax.div(me, 2)
    refs = (q_ref, k_ref, v_ref, sq_ref, rl_ref, du_ref, ru_ref, base_ref)

    @pl.loop(0, PAIRS)
    def _(i):
        pair = lax.rem(first_pair + i, PAIRS)

        @pl.when(i > 0)
        def _():
            send_pair(lax.rem(first_pair + i + PAIRS - 1, PAIRS))

        @pl.when((i >= 2) & (lax.rem(i, 2) == 0))
        def _():
            ring_step(lax.div(i, 2) - 1)

        pair_body(pair, refs, msg_ref, p_ref, o_ref)

    got_ref[me] = msg_ref[me]
    send_pair(lax.rem(first_pair + PAIRS - 1, PAIRS))

    @pl.loop(1, SP)
    def _(j):
        other = lax.rem(me + j, SP)
        remote(
            msg_ref.at[me], got_ref.at[other], msg_send.at[other], msg_recv.at[other], sp=other
        ).wait_recv()

    compose_chunks(lax.rem(me, 2) == 1, got_ref, zs_ref, group_ref)

    def send_state(chunk):
        return remote(
            zs_ref.at[chunk], zgot_ref.at[me], z_send.at[chunk], z_recv.at[me], sp=chunk
        )

    zgot_ref[me] = zs_ref[me]

    @pl.loop(1, SP)
    def _(j):
        send_state(lax.rem(me + j, SP)).start()

    @pl.loop(1, SP)
    def _(j):
        other = lax.rem(me + SP - j, SP)
        remote(
            zs_ref.at[me], zgot_ref.at[other], z_send.at[other], z_recv.at[other], sp=other
        ).wait_recv()

    @pl.loop(0, PAIRS)
    def _(i):
        pair_finish(i, zgot_ref, p_ref, o_ref, gain_ref, mix_ref)

    @pl.loop(0, 7)
    def _(s):
        near = lax.div(s, 2) + 1
        half0 = lax.rem(s, 2)
        for way in range(2):
            half = half0 if way == 0 else 1 - half0
            column = lax.rem(chip + (YN - near if way == 0 else near), YN) * 2 + 1 - core
            side(2 * s + way, column, half).wait_recv()

    for order in range(2):
        side(14 + order, partner, order).wait_recv()

    project(mix_ref, wall_ref, out_ref)

    @pl.loop(1, SP)
    def _(j):
        other = lax.rem(me + j, SP)
        send_message(other).wait_send()
        send_state(other).wait_send()

    @pl.loop(0, 7)
    def _(s):
        for way in range(2):
            ring(way, s, dp, 0).wait_send()
            side(2 * s + way, dp, 0).wait_send()

    for order in range(2):
        side(14 + order, dp, order).wait_send()


def per_device(query, key, value, decay_low, rate_low, decay_up, rate_up, base, gain, weight):
    vmem = pl.BlockSpec(memory_space=pltpu.VMEM)
    dma = pltpu.SemaphoreType.DMA
    out = pl.pallas_call(
        kernel,
        out_shape=jax.ShapeDtypeStruct((C, 2048), BF16),
        in_specs=[vmem] * 9 + [pl.BlockSpec(memory_space=pl.ANY)],
        out_specs=vmem,
        scratch_shapes=[
            pltpu.VMEM((C, C), BF16),
            pltpu.VMEM((SP, MSG, C), BF16),
            pltpu.VMEM((SP, MSG, C), BF16),
            pltpu.VMEM((4, 512, C), F32),
            pltpu.VMEM((SP, 32, C), BF16),
            pltpu.VMEM((SP, 32, C), BF16),
            pltpu.VMEM((PAIRS, C, 2 * C), BF16),
            pltpu.VMEM((PAIRS, C, C), F32),
            pltpu.VMEM((C, 2048), BF16),
            pltpu.VMEM((DPN, 2048, C), BF16),
            dma,
            dma((SP,)),
            dma((SP,)),
            dma((SP,)),
            dma((SP,)),
            dma((2, 7)),
            dma((2, 7)),
            dma((16,)),
            dma((16,)),
        ],
        compiler_params=pltpu.CompilerParams(
            collective_id=0, has_side_effects=True, vmem_limit_bytes=60 * 2**20
        ),
        name="mixer",
    )(
        query[0],
        key[0],
        value[0],
        decay_low[0],
        rate_low[0],
        decay_up,
        rate_up,
        base.reshape(PAIRS, C),
        gain.reshape(PAIRS, C),
        weight,
    )
    return out[None]


def solution(mesh):
    placed = (P("dp", "sp", None),) * 5 + (P(),) * 4 + (P(None, "dp"),)
    return jax.shard_map(
        per_device, mesh=mesh, in_specs=placed, out_specs=P("dp", "sp", None), check_vma=False
    )
```

profile of v0, /device:TPU:2, one launch (start us, length us, event | category | flops | bytes accessed | tf_op | source)
XLA Modules:
  0.0 103.0 jit_solution(15194719455875499279)
XLA Ops:
  0.0 101.1 %mixer.1 = bf16[128,2048]{1,0:T(8,128)(2,1)} custom-call(bf16[128,2048]{1,0:T(8,128)(2,1)} %bitcast.9, bf16[128,2048]{1,0:T(8,128)(2,1)} %bitcast.10, bf16[128,2048]{1,0:T(8,128)(2,1)} %bitcast.11, bf16[128,128]{1,0:T(8,128)(2,1)} %bitcast.12, bf16[128,128]{1,0:T(8,128)(2,1)} %bitcast.13, bf16[128,2048]{1,0:T(8,128)(2,1)} %du_ref.1, ...), custom_call_target="tpu_custom_call" | custom-call | tf_op jit(solution)/shard_map/mixer/pallas_call | solution.py:422
  101.1 1.9 %copy.12 = bf16[1,128,2048]{2,1,0:T(8,128)(2,1)} copy(bf16[1,128,2048]{2,1,0:T(8,128)(2,1)} %bitcast.8) | data formatting | bytes 1048576
where the time goes:
time: 103 us
  Pallas kernels  101 us (98%)
  local copies, waits for them, and re-layouts  1.88 us (2%)
    pallas_call x1, Pallas kernels, per_device(): pl.pallas_call(kernel, out_shape=jax.ShapeDtypeStruct((C, 2048), BF16), i...  101 us

commit v1 on v0

--- a/solution.py
+++ b/solution.py
@@ -84,72 +84,107 @@
     return f1, f2, g1, g2, f1 * from_start, f2 * from_start, g1 * to_end, g2 * to_end, jnp.exp(final)
 
 
-def pair_body(pair, refs, msg_ref, p_ref, o_ref):
-    q_ref, k_ref, v_ref, sq_ref, rl_ref, du_ref, ru_ref, base_ref = refs
+def invert_unit_lower(lows):
+    row, col = iotas()
+    differ = row ^ col
+    zero = jnp.zeros((C, C), BF16)
+    lane16 = lax.broadcasted_iota(jnp.int32, (16, C), 1)
+    row16 = lax.broadcasted_iota(jnp.int32, (16, C), 0)
+    inner = row16 ^ (lane16 & 15)
+
+    def gather(low):
+        out = low[0:16]
+        for b in range(1, 8):
+            out = jnp.where((lane16 >> 4) == b, low[16 * b : 16 * b + 16], out)
+        return out
+
+    def spread(small, size):
+        own = (row // size) == (col // size)
+        tiled = rows_of(*[small.astype(BF16)] * (C // size)) if size < C else small.astype(BF16)
+        return jnp.where(own, tiled, zero)
+
+    eye = jnp.where(inner == 0, 1.0, 0.0)
+    small = [eye - jnp.where(inner == 1, gather(low).astype(F32), 0.0) for low in lows]
+    size = 2
+    while size < 16:
+        level = (differ >= size) & (differ < 2 * size)
+        mid = [nn(s.astype(BF16), jnp.where(level, low, zero)).astype(BF16) for s, low in zip(small, lows)]
+        small = [s - nn(m, spread(s, 16)) for s, m in zip(small, mid)]
+        size *= 2
+    while size < C:
+        level = (differ >= size) & (differ < 2 * size)
+        even = (lax.broadcasted_iota(jnp.int32, (size, C), 1) & size) == 0
+        mid = [
+            nn(jnp.where(even, 0.0, s).astype(BF16), jnp.where(level, low, zero)).astype(BF16)
+            for s, low in zip(small, lows)
+        ]
+        corner = [nn(m, spread(s, size)) for s, m in zip(small, mid)]
+        small = [rows_of(jnp.where(even, s, 0.0), jnp.where(even, -c, s)) for s, c in zip(small, corner)]
+        size *= 2
+    return [s.astype(BF16) for s in small]
+
+
+def group_body(pairs, refs, msg_ref, p_ref, o_ref):
+    v_ref = refs[2]
     row, col = iotas()
     first = col < 64
     first_b = lax.broadcasted_iota(jnp.int32, (2 * C, C), 1) < 64
     strict = row > col
     within = row >= col
-    at = pl.ds(pl.multiple_of(pair * C, C), C)
-    f1, f2, g1, g2, es, qs, ke, ee, efin = pair_front(pair, *refs)
-    f_h, f_l = split(rows_of(f1, f2))
     zero2 = jnp.zeros((2 * C, C), BF16)
-    fa_h, fa_l = jnp.where(first_b, f_h, zero2), jnp.where(first_b, f_l, zero2)
-    fb_h, fb_l = jnp.where(first_b, zero2, f_h), jnp.where(first_b, zero2, f_l)
-    g_h, g_l = split(rows_of(g1, g2))
-    gg = lanes_of(g_h, g_h)
-    grams = [
-        nt(lanes_of(fa_h, fa_l), gg) + nt(fa_h, g_l),
-        nt(lanes_of(fb_h, fb_l), gg) + nt(fb_h, g_l),
+    zero1 = jnp.zeros((C, C), BF16)
+    ep, kp, rk, re, ends, v_rolls = [], [], [], [], [], []
+    for pair in pairs:
+        at = pl.ds(pl.multiple_of(pair * C, C), C)
+        f1, f2, g1, g2, es, qs, ke, ee, efin = pair_front(pair, *refs)
+        ends.append((es, qs, ke, ee, efin))
+        v_rolls.append(roll_half(v_ref[:, at].astype(F32)).astype(BF16))
+        f_h, f_l = split(rows_of(f1, f2))
+        g_h, g_l = split(rows_of(g1, g2))
+        gg = lanes_of(g_h, g_h)
+        for i in range(2):
+            a_h = jnp.where(first_b, f_h, zero2) if i == 0 else jnp.where(first_b, zero2, f_h)
+            a_l = jnp.where(first_b, f_l, zero2) if i == 0 else jnp.where(first_b, zero2, f_l)
+            g = nt(lanes_of(a_h, a_l), gg) + nt(a_h, g_l)
+            kp.append(split(jnp.where(strict, g[:C, :C], 0.0)))
+            ep.append(split(jnp.where(strict, g[:C, C:], 0.0)))
+            rk.append(split(jnp.where(within, g[C:, :C], 0.0)))
+            re.append(split(jnp.where(within, g[C:, C:], 0.0)))
+    heads = range(2 * len(pairs))
+    carried = [nn(lanes_of(*kp[n]), rows_of(v_rolls[n // 2], v_rolls[n // 2])) for n in heads]
+    xb = invert_unit_lower([e[0] for e in ep])
+    rhs = [
+        jnp.where(first, ends[n // 2][0], carried[n]) if n % 2 == 0 else jnp.where(first, carried[n], ends[n // 2][0])
+        for n in heads
     ]
-    v_roll = roll_half(v_ref[:, at].astype(F32)).astype(BF16)
-    zero1 = jnp.zeros((C, C), BF16)
-    eye = jnp.where(row == col, 1.0, 0.0)
-    ep, kp, rk, re, x = [], [], [], [], []
-    differ = row ^ col
-    for g in grams:
-        kp.append(split(jnp.where(strict, g[:C, :C], 0.0)))
-        ep.append(split(jnp.where(strict, g[:C, C:], 0.0)))
-        rk.append(split(jnp.where(within, g[C:, :C], 0.0)))
-        re.append(split(jnp.where(within, g[C:, C:], 0.0)))
-        x.append(eye - jnp.where(differ == 1, ep[-1][0].astype(F32), 0.0))
-    size = 2
-    while size < C:
-        level = (differ >= size) & (differ < 2 * size)
-        xb = [a.astype(BF16) for a in x]
-        mid = [nn(xb[i], jnp.where(level, ep[i][0], zero1)).astype(BF16) for i in range(2)]
-        x = [x[i] - nn(mid[i], xb[i]) for i in range(2)]
-        size *= 2
-    ee_t = split(ee.T)
-    ke_t = split(ke.T)
+    s0 = [nn(xb[n], rhs[n].astype(BF16)).astype(BF16) for n in heads]
+    resid = [rhs[n] - s0[n].astype(F32) - nn(lanes_of(*ep[n]), rows_of(s0[n], s0[n])) for n in heads]
+    sol = [s0[n].astype(F32) + nn(xb[n], resid[n].astype(BF16)) for n in heads]
     outs = []
-    for i in range(2):
-        mine = first if i == 0 else ~first
-        xb = x[i].astype(BF16)
-        carried = nn(lanes_of(*kp[i]), rows_of(v_roll, v_roll))
-        rhs = jnp.where(mine, es, carried)
-        s0 = nn(xb, rhs.astype(BF16)).astype(BF16)
-        resid = rhs - s0.astype(F32) - nn(lanes_of(*ep[i]), rows_of(s0, s0))
-        sol = s0.astype(F32) + nn(xb, resid.astype(BF16))
-        n_h, n_l = split(-sol)
-        v_mine = jnp.where(mine, zero1, v_roll)
+    for n in heads:
+        _, _, ke, ee, _ = ends[n // 2]
+        half = slice(64 * (n % 2), 64 * (n % 2) + 64)
+        ee_h, ee_l = split(ee.T[half])
+        ke_h, ke_l = split(ke.T[half])
+        n_h, n_l = split(-sol[n])
+        v_roll = v_rolls[n // 2]
+        v_mine = jnp.where(first, zero1, v_roll) if n % 2 == 0 else jnp.where(first, v_roll, zero1)
         w_h = rows_of(n_h, v_mine)
-        half = slice(64 * i, 64 * i + 64)
-        l_h = rows_of(lanes_of(ee_t[0][half], ke_t[0][half]), lanes_of(re[i][0], rk[i][0]))
-        l_l = rows_of(lanes_of(ee_t[1][half], ke_t[1][half]), lanes_of(re[i][1], rk[i][1]))
-        outs.append(nn(l_h, w_h) + nn(l_l, w_h) + nn(rows_of(ee_t[0][half], re[i][0]), n_l))
-    d_h, d_l = split(jnp.broadcast_to(efin, (16, C)))
+        l_h = rows_of(lanes_of(ee_h, ke_h), lanes_of(re[n][0], rk[n][0]))
+        l_l = rows_of(lanes_of(ee_l, ke_l), lanes_of(re[n][1], rk[n][1]))
+        outs.append(nn(l_h, w_h) + nn(l_l, w_h) + nn(rows_of(ee_h, re[n][0]), n_l))
     low_rows = lax.broadcasted_iota(jnp.int32, (16, C), 0) < 8
-    d_tile = jnp.where(low_rows, d_h, d_l)
-    for i in range(2):
-        msg_ref[2 * pair + i, pl.ds(0, 64), :] = outs[i][:64].astype(BF16)
-        msg_ref[2 * pair + i, pl.ds(64, 16), :] = d_tile
-    p_all = qs + jnp.where(first, outs[0][64:], outs[1][64:])
-    o_all = roll_half(jnp.where(first, outs[1][64:], outs[0][64:]))
-    p_h, p_l = split(p_all)
-    p_ref[pair] = lanes_of(p_h, p_l)
-    o_ref[pair] = o_all
+    for m, pair in enumerate(pairs):
+        d_h, d_l = split(jnp.broadcast_to(ends[m][4], (16, C)))
+        d_tile = jnp.where(low_rows, d_h, d_l)
+        for i in range(2):
+            msg_ref[2 * pair + i, pl.ds(0, 64), :] = outs[2 * m + i][:64].astype(BF16)
+            msg_ref[2 * pair + i, pl.ds(64, 16), :] = d_tile
+        p_all = ends[m][1] + jnp.where(first, outs[2 * m][64:], outs[2 * m + 1][64:])
+        o_all = roll_half(jnp.where(first, outs[2 * m + 1][64:], outs[2 * m][64:]))
+        p_h, p_l = split(p_all)
+        p_ref[pair] = lanes_of(p_h, p_l)
+        o_ref[pair] = o_all
 
 
 def compose_chunks(odd, msg_ref, zs_ref, g_ref):
@@ -200,24 +235,30 @@
     return nn(lhs, rows_of(z_h, z_h, z_l, zero))
 
 
-def pair_finish(pair, z_ref, p_ref, o_ref, gain_ref, mix_ref):
+GF = GROUP = 4
+
+
+def group_finish(pairs, z_ref, p_ref, o_ref, gain_ref, mix_ref):
     row, col = iotas()
     left = lax.broadcasted_iota(jnp.int32, (32, C), 1) < 64
-    za = z_ref[2 * pair].astype(F32)
-    zb = z_ref[2 * pair + 1].astype(F32)
-    zw = rows_of(
-        jnp.where(left, za, 0.0),
-        jnp.where(left, roll_half(za), 0.0),
-        jnp.where(left, 0.0, roll_half(zb)),
-        jnp.where(left, 0.0, zb),
-    ).astype(BF16)
-    read = o_ref[pair] + nn(p_ref[pair], rows_of(zw, zw))
     mean_w = jnp.where((row < 64) == (col < 64), 1.0 / 64, 0.0).astype(BF16)
     mean_w = rows_of(mean_w, mean_w)
-    centred = read - nn(lanes_of(*split(read)), mean_w)
-    var = nn(lanes_of(*split(centred * centred)), mean_w)
-    at = pl.ds(pl.multiple_of(pair * C, C), C)
-    mix_ref[:, at] = (centred * lax.rsqrt(var + 1.0) * gain_ref[pl.ds(pair, 1), :]).astype(BF16)
+    reads = []
+    for pair in pairs:
+        za = z_ref[2 * pair].astype(F32)
+        zb = z_ref[2 * pair + 1].astype(F32)
+        zw = rows_of(
+            jnp.where(left, za, 0.0),
+            jnp.where(left, roll_half(za), 0.0),
+            jnp.where(left, 0.0, roll_half(zb)),
+            jnp.where(left, 0.0, zb),
+        ).astype(BF16)
+        reads.append(o_ref[pair] + nn(p_ref[pair], rows_of(zw, zw)))
+    centred = [r - nn(lanes_of(*split(r)), mean_w) for r in reads]
+    var = [nn(lanes_of(*split(c * c)), mean_w) for c in centred]
+    for pair, c, v in zip(pairs, centred, var):
+        at = pl.ds(pl.multiple_of(pair * C, C), C)
+        mix_ref[:, at] = (c * lax.rsqrt(v + 1.0) * gain_ref[pl.ds(pair, 1), :]).astype(BF16)
 
 
 def project(mix_ref, w_ref, out_ref):
@@ -309,15 +350,14 @@
         side(14 + order, dp, order).start()
 
     def ring_step(s):
-        near = lax.div(s, 2) + 1
-        half0 = lax.rem(s, 2)
+        near = s // 2 + 1
+        half0 = s % 2
         for way in range(2):
             half = half0 if way == 0 else 1 - half0
             column = lax.rem(chip + (YN - near if way == 0 else near), YN) * 2 + core
             ring(way, s, column, half).wait_recv()
 
-            @pl.when(s < 5)
-            def _():
+            if not isinstance(s, int) or s < 5:
                 ring(way, s + 2, column, half).start()
 
             side(2 * s + way, column, half).start()
@@ -338,22 +378,28 @@
     first_pair = lax.div(me, 2)
     refs = (q_ref, k_ref, v_ref, sq_ref, rl_ref, du_ref, ru_ref, base_ref)
 
-    @pl.loop(0, PAIRS)
+    def pairs_of(i):
+        return [lax.rem(first_pair + GROUP * i + j, PAIRS) for j in range(GROUP)]
+
+    def send_group(i):
+        for pair in pairs_of(i):
+            send_pair(pair)
+
+    @pl.loop(0, PAIRS // GROUP)
     def _(i):
-        pair = lax.rem(first_pair + i, PAIRS)
-
         @pl.when(i > 0)
         def _():
-            send_pair(lax.rem(first_pair + i + PAIRS - 1, PAIRS))
-
-        @pl.when((i >= 2) & (lax.rem(i, 2) == 0))
+            send_group(i - 1)
+
+        @pl.when(i >= 2)
         def _():
-            ring_step(lax.div(i, 2) - 1)
-
-        pair_body(pair, refs, msg_ref, p_ref, o_ref)
+            ring_step(i - 2)
+
+        group_body(pairs_of(i), refs, msg_ref, p_ref, o_ref)
 
     got_ref[me] = msg_ref[me]
-    send_pair(lax.rem(first_pair + PAIRS - 1, PAIRS))
+    send_group(PAIRS // GROUP - 1)
+    ring_step(2)
 
     @pl.loop(1, SP)
     def _(j):
@@ -362,6 +408,7 @@
             msg_ref.at[me], got_ref.at[other], msg_send.at[other], msg_recv.at[other], sp=other
         ).wait_recv()
 
+    ring_step(3)
     compose_chunks(lax.rem(me, 2) == 1, got_ref, zs_ref, group_ref)
 
     def send_state(chunk):
@@ -374,6 +421,8 @@
     @pl.loop(1, SP)
     def _(j):
         send_state(lax.rem(me + j, SP)).start()
+
+    ring_step(4)
 
     @pl.loop(1, SP)
     def _(j):
@@ -382,9 +431,12 @@
             zs_ref.at[me], zgot_ref.at[other], z_send.at[other], z_recv.at[other], sp=other
         ).wait_recv()
 
-    @pl.loop(0, PAIRS)
+    @pl.loop(0, PAIRS // GROUP)
     def _(i):
-        pair_finish(i, zgot_ref, p_ref, o_ref, gain_ref, mix_ref)
+        group_finish([GROUP * i + j for j in range(GROUP)], zgot_ref, p_ref, o_ref, gain_ref, mix_ref)
+
+    ring_step(5)
+    ring_step(6)
 
     @pl.loop(0, 7)
     def _(s):

time: 103 us -> 69.9 us (0.68)
  the two profiles are of different devices: /device:TPU:2 before, /device:TPU:1 now
where the time goes in v1:
time: 69.9 us; the launch traced here: 69.6 us
  Pallas kernels  67.7 us (97%)
  local copies, waits for them, and re-layouts  1.88 us (3%)
    pallas_call x1, Pallas kernels, per_device(): pl.pallas_call(kernel, out_shape=jax.ShapeDtypeStruct((C, 2048), BF16), i...  67.7 us
    unnamed x1, local copies, waits for them, and re-layouts  1.88 us

profile of v1, /device:TPU:1, one launch (start us, length us, event | category | flops | bytes accessed | tf_op | source)
XLA Modules:
  0.0 69.6 jit_solution(2017954432942210217)
XLA Ops:
  0.0 67.7 %mixer.1 = bf16[128,2048]{1,0:T(8,128)(2,1)} custom-call(bf16[128,2048]{1,0:T(8,128)(2,1)} %bitcast.9, bf16[128,2048]{1,0:T(8,128)(2,1)} %bitcast.10, bf16[128,2048]{1,0:T(8,128)(2,1)} %bitcast.11, bf16[128,128]{1,0:T(8,128)(2,1)} %bitcast.12, bf16[128,128]{1,0:T(8,128)(2,1)} %bitcast.13, bf16[128,2048]{1,0:T(8,128)(2,1)} %du_ref.1, ...), custom_call_target="tpu_custom_call" | custom-call | tf_op jit(solution)/shard_map/mixer/pallas_call | solution.py:474
  67.7 1.9 %copy.12 = bf16[1,128,2048]{2,1,0:T(8,128)(2,1)} copy(bf16[1,128,2048]{2,1,0:T(8,128)(2,1)} %bitcast.8) | data formatting | bytes 1048576

commit v2 on v1

--- a/solution.py
+++ b/solution.py
@@ -104,13 +104,19 @@
         return jnp.where(own, tiled, zero)
 
     eye = jnp.where(inner == 0, 1.0, 0.0)
-    small = [eye - jnp.where(inner == 1, gather(low).astype(F32), 0.0) for low in lows]
-    size = 2
-    while size < 16:
-        level = (differ >= size) & (differ < 2 * size)
-        mid = [nn(s.astype(BF16), jnp.where(level, low, zero)).astype(BF16) for s, low in zip(small, lows)]
-        small = [s - nn(m, spread(s, 16)) for s, m in zip(small, mid)]
-        size *= 2
+    wide_row = lax.broadcasted_iota(jnp.int32, (C, 16 * C), 0)
+    wide_col = lax.broadcasted_iota(jnp.int32, (C, 16 * C), 1)
+    pick = (wide_row & 15) == (wide_col // C)
+    pick = jnp.where(pick & ((wide_row >> 4) == ((wide_col % C) >> 4)), 1.0, 0.0).astype(BF16)
+    packed = [gather(low) for low in lows]
+    columns = nn(rows_of(*packed), pick)
+    small = []
+    for n in range(len(lows)):
+        x = eye
+        for s in range(15):
+            x = x - columns[16 * n : 16 * n + 16, C * s : C * s + C] * x[s : s + 1]
+        small.append(x)
+    size = 16
     while size < C:
         level = (differ >= size) & (differ < 2 * size)
         even = (lax.broadcasted_iota(jnp.int32, (size, C), 1) & size) == 0
@@ -124,32 +130,35 @@
     return [s.astype(BF16) for s in small]
 
 
-def group_body(pairs, refs, msg_ref, p_ref, o_ref):
+def masked(x, i):
+    first = lax.broadcasted_iota(jnp.int32, x.shape, 1) < 64
+    zero = jnp.zeros(x.shape, x.dtype)
+    return jnp.where(first, x, zero) if i == 0 else jnp.where(first, zero, x)
+
+
+def group_states(pairs, refs, msg_ref, hold):
+    f_ref, g_ref, qs_ref, w_ref, n_ref = hold
     v_ref = refs[2]
     row, col = iotas()
     first = col < 64
-    first_b = lax.broadcasted_iota(jnp.int32, (2 * C, C), 1) < 64
     strict = row > col
-    within = row >= col
-    zero2 = jnp.zeros((2 * C, C), BF16)
-    zero1 = jnp.zeros((C, C), BF16)
-    ep, kp, rk, re, ends, v_rolls = [], [], [], [], [], []
+    ep, kp, ends, v_rolls = [], [], [], []
     for pair in pairs:
         at = pl.ds(pl.multiple_of(pair * C, C), C)
         f1, f2, g1, g2, es, qs, ke, ee, efin = pair_front(pair, *refs)
-        ends.append((es, qs, ke, ee, efin))
+        qs_ref[pair] = qs
+        f_ref[pair] = lanes_of(*split(f2))
+        ends.append((es, ke, ee, efin))
         v_rolls.append(roll_half(v_ref[:, at].astype(F32)).astype(BF16))
-        f_h, f_l = split(rows_of(f1, f2))
+        f_h, f_l = split(f1)
         g_h, g_l = split(rows_of(g1, g2))
+        g_ref[pair] = lanes_of(g_h, g_l)
         gg = lanes_of(g_h, g_h)
         for i in range(2):
-            a_h = jnp.where(first_b, f_h, zero2) if i == 0 else jnp.where(first_b, zero2, f_h)
-            a_l = jnp.where(first_b, f_l, zero2) if i == 0 else jnp.where(first_b, zero2, f_l)
+            a_h, a_l = masked(f_h, i), masked(f_l, i)
             g = nt(lanes_of(a_h, a_l), gg) + nt(a_h, g_l)
-            kp.append(split(jnp.where(strict, g[:C, :C], 0.0)))
-            ep.append(split(jnp.where(strict, g[:C, C:], 0.0)))
-            rk.append(split(jnp.where(within, g[C:, :C], 0.0)))
-            re.append(split(jnp.where(within, g[C:, C:], 0.0)))
+            kp.append(split(jnp.where(strict, g[:, :C], 0.0)))
+            ep.append(split(jnp.where(strict, g[:, C:], 0.0)))
     heads = range(2 * len(pairs))
     carried = [nn(lanes_of(*kp[n]), rows_of(v_rolls[n // 2], v_rolls[n // 2])) for n in heads]
     xb = invert_unit_lower([e[0] for e in ep])
@@ -160,31 +169,42 @@
     s0 = [nn(xb[n], rhs[n].astype(BF16)).astype(BF16) for n in heads]
     resid = [rhs[n] - s0[n].astype(F32) - nn(lanes_of(*ep[n]), rows_of(s0[n], s0[n])) for n in heads]
     sol = [s0[n].astype(F32) + nn(xb[n], resid[n].astype(BF16)) for n in heads]
-    outs = []
+    low_rows = lax.broadcasted_iota(jnp.int32, (16, C), 0) < 8
     for n in heads:
-        _, _, ke, ee, _ = ends[n // 2]
+        _, ke, ee, efin = ends[n // 2]
+        head = 2 * pairs[n // 2] + n % 2
         half = slice(64 * (n % 2), 64 * (n % 2) + 64)
         ee_h, ee_l = split(ee.T[half])
         ke_h, ke_l = split(ke.T[half])
         n_h, n_l = split(-sol[n])
-        v_roll = v_rolls[n // 2]
-        v_mine = jnp.where(first, zero1, v_roll) if n % 2 == 0 else jnp.where(first, v_roll, zero1)
-        w_h = rows_of(n_h, v_mine)
-        l_h = rows_of(lanes_of(ee_h, ke_h), lanes_of(re[n][0], rk[n][0]))
-        l_l = rows_of(lanes_of(ee_l, ke_l), lanes_of(re[n][1], rk[n][1]))
-        outs.append(nn(l_h, w_h) + nn(l_l, w_h) + nn(rows_of(ee_h, re[n][0]), n_l))
-    low_rows = lax.broadcasted_iota(jnp.int32, (16, C), 0) < 8
-    for m, pair in enumerate(pairs):
-        d_h, d_l = split(jnp.broadcast_to(ends[m][4], (16, C)))
-        d_tile = jnp.where(low_rows, d_h, d_l)
+        w_h = rows_of(n_h, masked(v_rolls[n // 2], 1 - n % 2))
+        w_ref[head] = w_h
+        n_ref[head] = n_l
+        out = nn(lanes_of(ee_h, ke_h), w_h) + nn(lanes_of(ee_l, ke_l), w_h) + nn(ee_h, n_l)
+        d_h, d_l = split(jnp.broadcast_to(efin, (16, C)))
+        msg_ref[head, pl.ds(0, 64), :] = out.astype(BF16)
+        msg_ref[head, pl.ds(64, 16), :] = jnp.where(low_rows, d_h, d_l)
+
+
+def group_reads(pairs, hold, p_ref, o_ref):
+    f_ref, g_ref, qs_ref, w_ref, n_ref = hold
+    row, col = iotas()
+    first = col < 64
+    within = row >= col
+    for pair in pairs:
+        g_h, g_l = g_ref[pair, :, pl.ds(0, C)], g_ref[pair, :, pl.ds(C, C)]
+        gg = lanes_of(g_h, g_h)
+        f_h, f_l = f_ref[pair, :, pl.ds(0, C)], f_ref[pair, :, pl.ds(C, C)]
+        outs = []
         for i in range(2):
-            msg_ref[2 * pair + i, pl.ds(0, 64), :] = outs[2 * m + i][:64].astype(BF16)
-            msg_ref[2 * pair + i, pl.ds(64, 16), :] = d_tile
-        p_all = ends[m][1] + jnp.where(first, outs[2 * m][64:], outs[2 * m + 1][64:])
-        o_all = roll_half(jnp.where(first, outs[2 * m + 1][64:], outs[2 * m][64:]))
-        p_h, p_l = split(p_all)
-        p_ref[pair] = lanes_of(p_h, p_l)
-        o_ref[pair] = o_all
+            a_h, a_l = masked(f_h, i), masked(f_l, i)
+            g = nt(lanes_of(a_h, a_l), gg) + nt(a_h, g_l)
+            rk_h, rk_l = split(jnp.where(within, g[:, :C], 0.0))
+            re_h, re_l = split(jnp.where(within, g[:, C:], 0.0))
+            w_h = w_ref[2 * pair + i]
+            outs.append(nn(lanes_of(re_h, rk_h), w_h) + nn(lanes_of(re_l, rk_l), w_h) + nn(re_h, n_ref[2 * pair + i]))
+        p_ref[pair] = lanes_of(*split(qs_ref[pair] + jnp.where(first, outs[0], outs[1])))
+        o_ref[pair] = roll_half(jnp.where(first, outs[1], outs[0]))
 
 
 def compose_chunks(odd, msg_ref, zs_ref, g_ref):
@@ -287,7 +307,7 @@
     ru_ref,
     base_ref,
     gain_ref,
-    w_ref,
+    weight_ref,
     out_ref,
     sq_ref,
     msg_ref,
@@ -299,6 +319,11 @@
     o_ref,
     mix_ref,
     wall_ref,
+    f_ref,
+    g_ref,
+    qs_ref,
+    w_ref,
+    n_ref,
     own_sem,
     msg_send,
     msg_recv,
@@ -327,11 +352,12 @@
 
     for other in (partner, up, down):
         pl.semaphore_signal(barrier, inc=1, device_id={"dp": other}, device_id_type=MESH)
-    own = pltpu.make_async_copy(w_ref, wall_ref.at[dp], own_sem)
+    own = pltpu.make_async_copy(weight_ref, wall_ref.at[dp], own_sem)
     own.start()
     sq_ref[...] = jnp.tanh(dl_ref[...].astype(F32)).astype(BF16)
-    own.wait()
-    pl.semaphore_wait(barrier, SP + 2)
+    with jax.named_scope('entry'):
+        own.wait()
+        pl.semaphore_wait(barrier, SP + 2)
 
     def piece(column, half):
         return wall_ref.at[column, pl.ds(half * 1024, 1024), :]
@@ -376,10 +402,11 @@
                 send_message(head).start()
 
     first_pair = lax.div(me, 2)
+    hold = (f_ref, g_ref, qs_ref, w_ref, n_ref)
     refs = (q_ref, k_ref, v_ref, sq_ref, rl_ref, du_ref, ru_ref, base_ref)
 
     def pairs_of(i):
-        return [lax.rem(first_pair + GROUP * i + j, PAIRS) for j in range(GROUP)]
+        return [lax.rem(first_pair + o, PAIRS) for o in (8 - 2 * i, 9 + 2 * i, 7 - 2 * i, 10 + 2 * i)]
 
     def send_group(i):
         for pair in pairs_of(i):
@@ -391,25 +418,37 @@
         def _():
             send_group(i - 1)
 
-        @pl.when(i >= 2)
-        def _():
+        with jax.named_scope('ringA'):
+          @pl.when(i >= 2)
+          def _():
             ring_step(i - 2)
 
-        group_body(pairs_of(i), refs, msg_ref, p_ref, o_ref)
+        with jax.named_scope('group'):
+            group_states(pairs_of(i), refs, msg_ref, hold)
 
     got_ref[me] = msg_ref[me]
     send_group(PAIRS // GROUP - 1)
-    ring_step(2)
-
-    @pl.loop(1, SP)
-    def _(j):
+    with jax.named_scope("ring2"):
+        ring_step(2)
+
+    def reads(i):
+        with jax.named_scope("reads"):
+            group_reads([GROUP * i + j for j in range(GROUP)], hold, p_ref, o_ref)
+
+    pl.loop(0, 2)(reads)
+
+    with jax.named_scope('msgwait'):
+     @pl.loop(1, SP)
+     def _(j):
         other = lax.rem(me + j, SP)
         remote(
             msg_ref.at[me], got_ref.at[other], msg_send.at[other], msg_recv.at[other], sp=other
         ).wait_recv()
 
-    ring_step(3)
-    compose_chunks(lax.rem(me, 2) == 1, got_ref, zs_ref, group_ref)
+    with jax.named_scope("ring3"):
+        ring_step(3)
+    with jax.named_scope('scan'):
+        compose_chunks(lax.rem(me, 2) == 1, got_ref, zs_ref, group_ref)
 
     def send_state(chunk):
         return remote(
@@ -422,24 +461,32 @@
     def _(j):
         send_state(lax.rem(me + j, SP)).start()
 
-    ring_step(4)
-
-    @pl.loop(1, SP)
-    def _(j):
+    with jax.named_scope("ring4"):
+        ring_step(4)
+
+    pl.loop(2, PAIRS // GROUP)(reads)
+
+    with jax.named_scope('zwait'):
+     @pl.loop(1, SP)
+     def _(j):
         other = lax.rem(me + SP - j, SP)
         remote(
             zs_ref.at[me], zgot_ref.at[other], z_send.at[other], z_recv.at[other], sp=other
         ).wait_recv()
 
-    @pl.loop(0, PAIRS // GROUP)
-    def _(i):
+    with jax.named_scope('finish'):
+     @pl.loop(0, PAIRS // GROUP)
+     def _(i):
         group_finish([GROUP * i + j for j in range(GROUP)], zgot_ref, p_ref, o_ref, gain_ref, mix_ref)
 
-    ring_step(5)
-    ring_step(6)
-
-    @pl.loop(0, 7)
-    def _(s):
+    with jax.named_scope("ring5"):
+        ring_step(5)
+    with jax.named_scope("ring6"):
+        ring_step(6)
+
+    with jax.named_scope('sidewait'):
+     @pl.loop(0, 7)
+     def _(s):
         near = lax.div(s, 2) + 1
         half0 = lax.rem(s, 2)
         for way in range(2):
@@ -450,10 +497,12 @@
     for order in range(2):
         side(14 + order, partner, order).wait_recv()
 
-    project(mix_ref, wall_ref, out_ref)
-
-    @pl.loop(1, SP)
-    def _(j):
+    with jax.named_scope('project'):
+        project(mix_ref, wall_ref, out_ref)
+
+    with jax.named_scope('tail'):
+     @pl.loop(1, SP)
+     def _(j):
         other = lax.rem(me + j, SP)
         send_message(other).wait_send()
         send_state(other).wait_send()
@@ -487,6 +536,11 @@
             pltpu.VMEM((PAIRS, C, C), F32),
             pltpu.VMEM((C, 2048), BF16),
             pltpu.VMEM((DPN, 2048, C), BF16),
+            pltpu.VMEM((PAIRS, C, 2 * C), BF16),
+            pltpu.VMEM((PAIRS, 2 * C, 2 * C), BF16),
+            pltpu.VMEM((PAIRS, C, C), F32),
+            pltpu.VMEM((SP, 2 * C, C), BF16),
+            pltpu.VMEM((SP, C, C), BF16),
             dma,
             dma((SP,)),
             dma((SP,)),

time: 69.9 us -> 67.5 us (0.966)
  Pallas kernels: 67.7 us -> 65.4 us
    pallas_call x1, Pallas kernels: 67.7 us -> 65.4 us  [per_device(): pl.pallas_call(kernel, out_shape=jax.ShapeDtypeStruct((C, 2048), BF16), i...]
where the time goes in v2:
time: 67.5 us; the launch traced here: 67.3 us
  Pallas kernels  65.4 us (97%)
  local copies, waits for them, and re-layouts  1.88 us (3%)
    pallas_call x1, Pallas kernels, per_device(): pl.pallas_call(kernel, out_shape=jax.ShapeDtypeStruct((C, 2048), BF16), i...  65.4 us
    unnamed x1, local copies, waits for them, and re-layouts  1.88 us

profile of v2, /device:TPU:1, one launch (start us, length us, event | category | flops | bytes accessed | tf_op | source)
XLA Modules:
  0.0 67.3 jit_solution(7823254177689655570)
XLA Ops:
  0.0 65.4 %mixer.1 = bf16[128,2048]{1,0:T(8,128)(2,1)} custom-call(bf16[128,2048]{1,0:T(8,128)(2,1)} %bitcast.9, bf16[128,2048]{1,0:T(8,128)(2,1)} %bitcast.10, bf16[128,2048]{1,0:T(8,128)(2,1)} %bitcast.11, bf16[128,128]{1,0:T(8,128)(2,1)} %bitcast.12, bf16[128,128]{1,0:T(8,128)(2,1)} %bitcast.13, bf16[128,2048]{1,0:T(8,128)(2,1)} %du_ref.1, ...), custom_call_target="tpu_custom_call" | custom-call | tf_op jit(solution)/shard_map/mixer/pallas_call | solution.py:523
  65.4 1.9 %copy.12 = bf16[1,128,2048]{2,1,0:T(8,128)(2,1)} copy(bf16[1,128,2048]{2,1,0:T(8,128)(2,1)} %bitcast.8) | data formatting | bytes 1048576

commit v3 on v2

--- a/solution.py
+++ b/solution.py
@@ -13,6 +13,8 @@
 DPN = 16
 YN = 8
 MSG = 80
+WHOLE = 1536
+QUARTER = (2048 - WHOLE) // 4
 DECAY_SCALE = 0.6065306597126334
 MESH = pl.DeviceIdType.MESH
 
@@ -281,14 +283,12 @@
         mix_ref[:, at] = (c * lax.rsqrt(v + 1.0) * gain_ref[pl.ds(pair, 1), :]).astype(BF16)
 
 
-def project(mix_ref, w_ref, out_ref):
-    @pl.loop(0, YN)
-    def _(y):
-        acc = jnp.zeros((C, 2 * C), F32)
-        for k in range(8):
-            w = lanes_of(w_ref[2 * y, pl.ds(256 * k, 256), :], w_ref[2 * y + 1, pl.ds(256 * k, 256), :])
-            acc = acc + nn(mix_ref[:, pl.ds(256 * k, 256)], w)
-        out_ref[:, pl.ds(pl.multiple_of(y * 256, 256), 256)] = acc.astype(BF16)
+def project(slot, mix_ref, w_ref, done_ref):
+    acc = jnp.zeros((C, 2 * C), F32)
+    for k in range(8):
+        at = pl.ds(256 * k, 256)
+        acc = acc + nn(mix_ref[:, at], lanes_of(w_ref[0, slot, at, :], w_ref[1, slot, at, :]))
+    done_ref[slot] = acc.astype(BF16)
 
 
 def remote(src, dst, send, recv, **where):
@@ -298,6 +298,17 @@
 
 
 def kernel(
+    q_in,
+    k_in,
+    v_in,
+    dl_in,
+    rl_in,
+    du_in,
+    ru_in,
+    base_in,
+    gain_in,
+    weight_ref,
+    out_ref,
     q_ref,
     k_ref,
     v_ref,
@@ -307,8 +318,9 @@
     ru_ref,
     base_ref,
     gain_ref,
-    weight_ref,
-    out_ref,
+    done_ref,
+    in_sem,
+    out_sem,
     sq_ref,
     msg_ref,
     got_ref,
@@ -331,6 +343,8 @@
     z_recv,
     ring_send,
     ring_recv,
+    quarter_send,
+    quarter_recv,
     side_send,
     side_recv,
 ):
@@ -342,6 +356,22 @@
     up = lax.rem(dp + 2, DPN)
     down = lax.rem(dp + DPN - 2, DPN)
 
+    inputs = [
+        pltpu.make_async_copy(src, dst, in_sem.at[n])
+        for n, (src, dst) in enumerate(
+            (
+                (dl_in, dl_ref),
+                (rl_in, rl_ref),
+                (du_in, du_ref),
+                (ru_in, ru_ref),
+                (base_in, base_ref),
+                (gain_in, gain_ref),
+                (k_in, k_ref),
+                (q_in, q_ref),
+                (v_in, v_ref),
+            )
+        )
+    ]
     barrier = pltpu.get_barrier_semaphore()
 
     @pl.loop(1, SP)
@@ -352,41 +382,74 @@
 
     for other in (partner, up, down):
         pl.semaphore_signal(barrier, inc=1, device_id={"dp": other}, device_id_type=MESH)
-    own = pltpu.make_async_copy(weight_ref, wall_ref.at[dp], own_sem)
+    own = pltpu.make_async_copy(weight_ref, wall_ref.at[core, 0], own_sem)
     own.start()
+    for copy in inputs:
+        copy.start()
+    inputs[0].wait()
     sq_ref[...] = jnp.tanh(dl_ref[...].astype(F32)).astype(BF16)
-    with jax.named_scope('entry'):
+    with jax.named_scope("entry"):
         own.wait()
+        for copy in inputs[1:]:
+            copy.wait()
         pl.semaphore_wait(barrier, SP + 2)
 
-    def piece(column, half):
-        return wall_ref.at[column, pl.ds(half * 1024, 1024), :]
-
-    def ring(way, order, column, half):
-        ref = piece(column, half)
-        return remote(ref, ref, ring_send.at[way, order], ring_recv.at[way, order], dp=(up, down)[way])
-
-    def side(slot, column, half):
-        ref = piece(column, half)
+    across = lax.rem(me, 4)
+    def rows(slot, start, count):
+        return wall_ref.at[core, slot, pl.ds(pl.multiple_of(start, QUARTER // 2), count), :]
+
+    def ring(way, order):
+        near = order // 2
+        half = order % 2 if way == 0 else 1 - order % 2
+        src, dst = ((YN - near) % YN, YN - 1 - near) if way == 0 else (near, near + 1)
+        spans = ((WHOLE // 2 * half, WHOLE // 2), (WHOLE + QUARTER * across + QUARTER // 2 * half, QUARTER // 2))
+        return [
+            remote(
+                rows(src, *spans[kind]),
+                rows(dst, *spans[kind]),
+                ring_send.at[kind, way, order],
+                ring_recv.at[kind, way, order],
+                dp=(up, down)[way],
+            )
+            for kind in range(2)
+        ]
+
+    def quarter(hop, slot):
+        ref = rows(slot, WHOLE + QUARTER * across, QUARTER)
+        there = me - across + lax.rem(across + hop + 1, 4)
+        return remote(ref, ref, quarter_send.at[hop, slot], quarter_recv.at[hop, slot], sp=there)
+
+    def side(slot, to_me=False):
+        start, count = ((0, WHOLE) if slot < YN else (WHOLE, 2048 - WHOLE)) if slot in (4, YN) else (0, 2048)
+        ref = wall_ref.at[1 - core if to_me else core, slot % YN if slot < YN else 4, pl.ds(start, count), :]
         return remote(ref, ref, side_send.at[slot], side_recv.at[slot], dp=partner)
 
-    for order in range(2):
-        ring(0, order, dp, order).start()
-        ring(1, order, dp, 1 - order).start()
-        side(14 + order, dp, order).start()
-
     def ring_step(s):
-        near = s // 2 + 1
-        half0 = s % 2
-        for way in range(2):
-            half = half0 if way == 0 else 1 - half0
-            column = lax.rem(chip + (YN - near if way == 0 else near), YN) * 2 + core
-            ring(way, s, column, half).wait_recv()
-
-            if not isinstance(s, int) or s < 5:
-                ring(way, s + 2, column, half).start()
-
-            side(2 * s + way, column, half).start()
+        with jax.named_scope("ring" + str(s)):
+            for way in range(2):
+                for copy in ring(way, s):
+                    copy.wait_recv()
+                if s < 5:
+                    for copy in ring(way, s + 2):
+                        copy.start()
+
+    def share(*slots):
+        for slot in slots:
+            for hop in range(3):
+                quarter(hop, slot).start()
+
+    def complete(*slots):
+        with jax.named_scope("complete"):
+            for slot in slots:
+                for hop in range(3):
+                    quarter(hop, slot).wait_recv()
+                side(YN if slot == 4 else slot).start()
+
+    for way in range(2):
+        for order in range(2):
+            for copy in ring(way, order):
+                copy.start()
+    side(0).start()
 
     def send_message(head):
         return remote(
@@ -418,24 +481,31 @@
         def _():
             send_group(i - 1)
 
-        with jax.named_scope('ringA'):
-          @pl.when(i >= 2)
-          def _():
-            ring_step(i - 2)
+        @pl.when(i == 2)
+        def _():
+            ring_step(0)
+
+        @pl.when(i == 3)
+        def _():
+            ring_step(1)
+            share(7, 1)
 
         with jax.named_scope('group'):
             group_states(pairs_of(i), refs, msg_ref, hold)
 
     got_ref[me] = msg_ref[me]
     send_group(PAIRS // GROUP - 1)
-    with jax.named_scope("ring2"):
-        ring_step(2)
+    ring_step(2)
 
     def reads(i):
         with jax.named_scope("reads"):
             group_reads([GROUP * i + j for j in range(GROUP)], hold, p_ref, o_ref)
 
-    pl.loop(0, 2)(reads)
+    reads(0)
+    complete(7, 1)
+    reads(1)
+    ring_step(3)
+    share(6, 2)
 
     with jax.named_scope('msgwait'):
      @pl.loop(1, SP)
@@ -445,8 +515,6 @@
             msg_ref.at[me], got_ref.at[other], msg_send.at[other], msg_recv.at[other], sp=other
         ).wait_recv()
 
-    with jax.named_scope("ring3"):
-        ring_step(3)
     with jax.named_scope('scan'):
         compose_chunks(lax.rem(me, 2) == 1, got_ref, zs_ref, group_ref)
 
@@ -457,75 +525,104 @@
 
     zgot_ref[me] = zs_ref[me]
 
-    @pl.loop(1, SP)
+    send_state(lax.rem(me + 16, SP)).start()
+
+    @pl.loop(1, 16)
     def _(j):
-        send_state(lax.rem(me + j, SP)).start()
-
-    with jax.named_scope("ring4"):
-        ring_step(4)
-
-    pl.loop(2, PAIRS // GROUP)(reads)
-
-    with jax.named_scope('zwait'):
-     @pl.loop(1, SP)
-     def _(j):
-        other = lax.rem(me + SP - j, SP)
-        remote(
-            zs_ref.at[me], zgot_ref.at[other], z_send.at[other], z_recv.at[other], sp=other
-        ).wait_recv()
-
-    with jax.named_scope('finish'):
-     @pl.loop(0, PAIRS // GROUP)
-     def _(i):
-        group_finish([GROUP * i + j for j in range(GROUP)], zgot_ref, p_ref, o_ref, gain_ref, mix_ref)
-
-    with jax.named_scope("ring5"):
-        ring_step(5)
-    with jax.named_scope("ring6"):
-        ring_step(6)
-
-    with jax.named_scope('sidewait'):
-     @pl.loop(0, 7)
-     def _(s):
-        near = lax.div(s, 2) + 1
-        half0 = lax.rem(s, 2)
+        send_state(lax.rem(me + 16 + j, SP)).start()
+        send_state(lax.rem(me + 16 - j, SP)).start()
+
+    reads(2)
+    ring_step(4)
+    complete(6, 2)
+    reads(3)
+
+    ring_step(5)
+    share(5, 3)
+
+    def wait_state(head):
+        @pl.when(head != me)
+        def _():
+            remote(
+                zs_ref.at[me], zgot_ref.at[head], z_send.at[head], z_recv.at[head], sp=head
+            ).wait_recv()
+
+    def finish(i):
+        with jax.named_scope("zwait"):
+            for pair in pairs_of(i):
+                wait_state(2 * pair)
+                wait_state(2 * pair + 1)
+        with jax.named_scope("finish"):
+            group_finish(pairs_of(i), zgot_ref, p_ref, o_ref, gain_ref, mix_ref)
+
+    pl.loop(0, 2)(finish)
+    ring_step(6)
+    share(4)
+    side(4).start()
+    complete(5, 3)
+    pl.loop(2, PAIRS // GROUP)(finish)
+
+    def put_out(slot):
+        at = pl.ds(pl.multiple_of(lax.rem(chip + slot, YN) * 256, 256), 256)
+        return pltpu.make_async_copy(done_ref.at[slot], out_ref.at[:, at], out_sem.at[slot])
+
+    def project_slots(*slots):
+        for slot in slots:
+            side(slot, True).wait_recv()
+            if slot == 4:
+                side(YN, True).wait_recv()
+        with jax.named_scope("project"):
+            for slot in slots:
+                project(slot, mix_ref, wall_ref, done_ref)
+                put_out(slot).start()
+
+    project_slots(0, 7, 1)
+    complete(4)
+    project_slots(6, 2, 5, 3)
+    project_slots(4)
+    with jax.named_scope("outwait"):
+        for slot in range(YN):
+            put_out(slot).wait()
+
+    with jax.named_scope("tail"):
+        @pl.loop(1, SP)
+        def _(j):
+            other = lax.rem(me + j, SP)
+            send_message(other).wait_send()
+            send_state(other).wait_send()
+
+    with jax.named_scope("sent"):
         for way in range(2):
-            half = half0 if way == 0 else 1 - half0
-            column = lax.rem(chip + (YN - near if way == 0 else near), YN) * 2 + 1 - core
-            side(2 * s + way, column, half).wait_recv()
-
-    for order in range(2):
-        side(14 + order, partner, order).wait_recv()
-
-    with jax.named_scope('project'):
-        project(mix_ref, wall_ref, out_ref)
-
-    with jax.named_scope('tail'):
-     @pl.loop(1, SP)
-     def _(j):
-        other = lax.rem(me + j, SP)
-        send_message(other).wait_send()
-        send_state(other).wait_send()
-
-    @pl.loop(0, 7)
-    def _(s):
-        for way in range(2):
-            ring(way, s, dp, 0).wait_send()
-            side(2 * s + way, dp, 0).wait_send()
-
-    for order in range(2):
-        side(14 + order, dp, order).wait_send()
+            for order in range(7):
+                for copy in ring(way, order):
+                    copy.wait_send()
+        for slot in range(1, YN):
+            for hop in range(3):
+                quarter(hop, slot).wait_send()
+        for slot in range(YN + 1):
+            side(slot).wait_send()
 
 
 def per_device(query, key, value, decay_low, rate_low, decay_up, rate_up, base, gain, weight):
-    vmem = pl.BlockSpec(memory_space=pltpu.VMEM)
     dma = pltpu.SemaphoreType.DMA
     out = pl.pallas_call(
         kernel,
         out_shape=jax.ShapeDtypeStruct((C, 2048), BF16),
-        in_specs=[vmem] * 9 + [pl.BlockSpec(memory_space=pl.ANY)],
-        out_specs=vmem,
+        in_specs=[pl.BlockSpec(memory_space=pl.ANY)] * 10,
+        out_specs=pl.BlockSpec(memory_space=pl.ANY),
         scratch_shapes=[
+            pltpu.VMEM((C, 2048), BF16),
+            pltpu.VMEM((C, 2048), BF16),
+            pltpu.VMEM((C, 2048), BF16),
+            pltpu.VMEM((C, C), BF16),
+            pltpu.VMEM((C, C), BF16),
+            pltpu.VMEM((C, 2048), BF16),
+            pltpu.VMEM((C, 2048), BF16),
+            pltpu.VMEM((PAIRS, C), F32),
+            pltpu.VMEM((PAIRS, C), F32),
+            pltpu.VMEM((YN, C, 2 * C), BF16),
+            dma((9,)),
+            dma((YN,)),
             pltpu.VMEM((C, C), BF16),
             pltpu.VMEM((SP, MSG, C), BF16),
             pltpu.VMEM((SP, MSG, C), BF16),
@@ -535,7 +632,7 @@
             pltpu.VMEM((PAIRS, C, 2 * C), BF16),
             pltpu.VMEM((PAIRS, C, C), F32),
             pltpu.VMEM((C, 2048), BF16),
-            pltpu.VMEM((DPN, 2048, C), BF16),
+            pltpu.VMEM((2, YN, 2048, C), BF16),
             pltpu.VMEM((PAIRS, C, 2 * C), BF16),
             pltpu.VMEM((PAIRS, 2 * C, 2 * C), BF16),
             pltpu.VMEM((PAIRS, C, C), F32),
@@ -546,10 +643,12 @@
             dma((SP,)),
             dma((SP,)),
             dma((SP,)),
-            dma((2, 7)),
-            dma((2, 7)),
-            dma((16,)),
-            dma((16,)),
+            dma((2, 2, 7)),
+            dma((2, 2, 7)),
+            dma((3, YN)),
+            dma((3, YN)),
+            dma((YN + 1,)),
+            dma((YN + 1,)),
         ],
         compiler_params=pltpu.CompilerParams(
             collective_id=0, has_side_effects=True, vmem_limit_bytes=60 * 2**20

time: 67.5 us -> 61.2 us (0.907)
  Pallas kernels: 65.4 us -> 59.1 us
    pallas_call x1, Pallas kernels: 65.4 us -> 59.1 us  [per_device(): pl.pallas_call(kernel, out_shape=jax.ShapeDtypeStruct((C, 2048), BF16), i...]
where the time goes in v3:
time: 61.2 us; the launch traced here: 61 us
  Pallas kernels  59.1 us (97%)
  local copies, waits for them, and re-layouts  1.88 us (3%)
    pallas_call x1, Pallas kernels, per_device(): pl.pallas_call(kernel, out_shape=jax.ShapeDtypeStruct((C, 2048), BF16), i...  59.1 us
    unnamed x1, local copies, waits for them, and re-layouts  1.88 us

profile of v3, /device:TPU:1, one launch (start us, length us, event | category | flops | bytes accessed | tf_op | source)
XLA Modules:
  0.0 61.0 jit_solution(8589949892291930301)
XLA Ops:
  0.0 59.1 %mixer.1 = bf16[128,2048]{1,0:T(8,128)(2,1)} custom-call(bf16[128,2048]{1,0:T(8,128)(2,1)} %bitcast.9, bf16[128,2048]{1,0:T(8,128)(2,1)} %bitcast.10, bf16[128,2048]{1,0:T(8,128)(2,1)} %bitcast.11, bf16[128,128]{1,0:T(8,128)(2,1)} %bitcast.12, bf16[128,128]{1,0:T(8,128)(2,1)} %bitcast.13, bf16[128,2048]{1,0:T(8,128)(2,1)} %du_in.1, bf16[128,2048]{1,0:T(8,128)(2,1)} %ru_in.1, ...), custom_call_target="tpu_custom_call" | custom-call | tf_op jit(solution)/shard_map/mixer/pallas_call | solution.py:608
  59.1 1.9 %copy.12 = bf16[1,128,2048]{2,1,0:T(8,128)(2,1)} copy(bf16[1,128,2048]{2,1,0:T(8,128)(2,1)} %bitcast.8) | data formatting | bytes 1048576

commit v4 on v3

--- a/solution.py
+++ b/solution.py
@@ -13,8 +13,8 @@
 DPN = 16
 YN = 8
 MSG = 80
-WHOLE = 1536
-QUARTER = (2048 - WHOLE) // 4
+WHOLE = 512
+PART = (2048 - WHOLE) // 4
 DECAY_SCALE = 0.6065306597126334
 MESH = pl.DeviceIdType.MESH
 
@@ -138,6 +138,13 @@
     return jnp.where(first, x, zero) if i == 0 else jnp.where(first, zero, x)
 
 
+def grams_of(f_h, f_l, gg, g_l):
+    high = rows_of(masked(f_h, 0), masked(f_h, 1))
+    low = rows_of(masked(f_l, 0), masked(f_l, 1))
+    g = nt(lanes_of(high, low), gg) + nt(high, g_l)
+    return g[:C], g[C:]
+
+
 def group_states(pairs, refs, msg_ref, hold):
     f_ref, g_ref, qs_ref, w_ref, n_ref = hold
     v_ref = refs[2]
@@ -156,9 +163,7 @@
         g_h, g_l = split(rows_of(g1, g2))
         g_ref[pair] = lanes_of(g_h, g_l)
         gg = lanes_of(g_h, g_h)
-        for i in range(2):
-            a_h, a_l = masked(f_h, i), masked(f_l, i)
-            g = nt(lanes_of(a_h, a_l), gg) + nt(a_h, g_l)
+        for g in grams_of(f_h, f_l, gg, g_l):
             kp.append(split(jnp.where(strict, g[:, :C], 0.0)))
             ep.append(split(jnp.where(strict, g[:, C:], 0.0)))
     heads = range(2 * len(pairs))
@@ -198,9 +203,7 @@
         gg = lanes_of(g_h, g_h)
         f_h, f_l = f_ref[pair, :, pl.ds(0, C)], f_ref[pair, :, pl.ds(C, C)]
         outs = []
-        for i in range(2):
-            a_h, a_l = masked(f_h, i), masked(f_l, i)
-            g = nt(lanes_of(a_h, a_l), gg) + nt(a_h, g_l)
+        for i, g in enumerate(grams_of(f_h, f_l, gg, g_l)):
             rk_h, rk_l = split(jnp.where(within, g[:, :C], 0.0))
             re_h, re_l = split(jnp.where(within, g[:, C:], 0.0))
             w_h = w_ref[2 * pair + i]
@@ -343,8 +346,8 @@
     z_recv,
     ring_send,
     ring_recv,
-    quarter_send,
-    quarter_recv,
+    swap_send,
+    swap_recv,
     side_send,
     side_recv,
 ):
@@ -395,14 +398,16 @@
         pl.semaphore_wait(barrier, SP + 2)
 
     across = lax.rem(me, 4)
+    parity = lax.rem(across, 2)
+
     def rows(slot, start, count):
-        return wall_ref.at[core, slot, pl.ds(pl.multiple_of(start, QUARTER // 2), count), :]
+        return wall_ref.at[core, slot, pl.ds(pl.multiple_of(start, 16), count), :]
 
     def ring(way, order):
         near = order // 2
         half = order % 2 if way == 0 else 1 - order % 2
         src, dst = ((YN - near) % YN, YN - 1 - near) if way == 0 else (near, near + 1)
-        spans = ((WHOLE // 2 * half, WHOLE // 2), (WHOLE + QUARTER * across + QUARTER // 2 * half, QUARTER // 2))
+        spans = ((WHOLE // 2 * half, WHOLE // 2), (WHOLE + 2 * PART * parity + PART * half, PART))
         return [
             remote(
                 rows(src, *spans[kind]),
@@ -414,10 +419,10 @@
             for kind in range(2)
         ]
 
-    def quarter(hop, slot):
-        ref = rows(slot, WHOLE + QUARTER * across, QUARTER)
-        there = me - across + lax.rem(across + hop + 1, 4)
-        return remote(ref, ref, quarter_send.at[hop, slot], quarter_recv.at[hop, slot], sp=there)
+    def swap(hop, slot):
+        ref = rows(slot, WHOLE + 2 * PART * parity + PART * hop, PART)
+        there = me - across + lax.rem(across + 1 + 2 * hop, 4)
+        return remote(ref, ref, swap_send.at[hop, slot], swap_recv.at[hop, slot], sp=there)
 
     def side(slot, to_me=False):
         start, count = ((0, WHOLE) if slot < YN else (WHOLE, 2048 - WHOLE)) if slot in (4, YN) else (0, 2048)
@@ -435,14 +440,14 @@
 
     def share(*slots):
         for slot in slots:
-            for hop in range(3):
-                quarter(hop, slot).start()
+            for hop in range(2):
+                swap(hop, slot).start()
 
     def complete(*slots):
         with jax.named_scope("complete"):
             for slot in slots:
-                for hop in range(3):
-                    quarter(hop, slot).wait_recv()
+                for hop in range(2):
+                    swap(hop, slot).wait_recv()
                 side(YN if slot == 4 else slot).start()
 
     for way in range(2):
@@ -502,7 +507,6 @@
             group_reads([GROUP * i + j for j in range(GROUP)], hold, p_ref, o_ref)
 
     reads(0)
-    complete(7, 1)
     reads(1)
     ring_step(3)
     share(6, 2)
@@ -532,10 +536,10 @@
         send_state(lax.rem(me + 16 + j, SP)).start()
         send_state(lax.rem(me + 16 - j, SP)).start()
 
+    ring_step(4)
     reads(2)
-    ring_step(4)
-    complete(6, 2)
     reads(3)
+    complete(7, 1)
 
     ring_step(5)
     share(5, 3)
@@ -559,8 +563,9 @@
     ring_step(6)
     share(4)
     side(4).start()
+    complete(6, 2)
+    pl.loop(2, PAIRS // GROUP)(finish)
     complete(5, 3)
-    pl.loop(2, PAIRS // GROUP)(finish)
 
     def put_out(slot):
         at = pl.ds(pl.multiple_of(lax.rem(chip + slot, YN) * 256, 256), 256)
@@ -597,8 +602,8 @@
                 for copy in ring(way, order):
                     copy.wait_send()
         for slot in range(1, YN):
-            for hop in range(3):
-                quarter(hop, slot).wait_send()
+            for hop in range(2):
+                swap(hop, slot).wait_send()
         for slot in range(YN + 1):
             side(slot).wait_send()
 
@@ -645,8 +650,8 @@
             dma((SP,)),
             dma((2, 2, 7)),
             dma((2, 2, 7)),
-            dma((3, YN)),
-            dma((3, YN)),
+            dma((2, YN)),
+            dma((2, YN)),
             dma((YN + 1,)),
             dma((YN + 1,)),
         ],

time: 61.2 us -> 58.6 us (0.958)
  Pallas kernels: 59.1 us -> 56.5 us
    pallas_call x1, Pallas kernels: 59.1 us -> 56.5 us  [per_device(): pl.pallas_call(kernel, out_shape=jax.ShapeDtypeStruct((C, 2048), BF16), i...]
where the time goes in v4:
time: 58.6 us; the launch traced here: 58.4 us
  Pallas kernels  56.5 us (96%)
  local copies, waits for them, and re-layouts  1.88 us (3%)
    pallas_call x1, Pallas kernels, per_device(): pl.pallas_call(kernel, out_shape=jax.ShapeDtypeStruct((C, 2048), BF16), i...  56.5 us
    unnamed x1, local copies, waits for them, and re-layouts  1.88 us

profile of v4, /device:TPU:1, one launch (start us, length us, event | category | flops | bytes accessed | tf_op | source)
XLA Modules:
  0.0 58.4 jit_solution(6568320425996273796)
XLA Ops:
  0.0 56.5 %mixer.1 = bf16[128,2048]{1,0:T(8,128)(2,1)} custom-call(bf16[128,2048]{1,0:T(8,128)(2,1)} %bitcast.9, bf16[128,2048]{1,0:T(8,128)(2,1)} %bitcast.10, bf16[128,2048]{1,0:T(8,128)(2,1)} %bitcast.11, bf16[128,128]{1,0:T(8,128)(2,1)} %bitcast.12, bf16[128,128]{1,0:T(8,128)(2,1)} %bitcast.13, bf16[128,2048]{1,0:T(8,128)(2,1)} %du_in.1, bf16[128,2048]{1,0:T(8,128)(2,1)} %ru_in.1, ...), custom_call_target="tpu_custom_call" | custom-call | tf_op jit(solution)/shard_map/mixer/pallas_call | solution.py:613
  56.6 1.9 %copy.12 = bf16[1,128,2048]{2,1,0:T(8,128)(2,1)} copy(bf16[1,128,2048]{2,1,0:T(8,128)(2,1)} %bitcast.8) | data formatting | bytes 1048576

commit v5 on v4

--- a/solution.py
+++ b/solution.py
@@ -537,9 +537,9 @@
         send_state(lax.rem(me + 16 - j, SP)).start()
 
     ring_step(4)
+    complete(7, 1)
     reads(2)
     reads(3)
-    complete(7, 1)
 
     ring_step(5)
     share(5, 3)
@@ -559,11 +559,12 @@
         with jax.named_scope("finish"):
             group_finish(pairs_of(i), zgot_ref, p_ref, o_ref, gain_ref, mix_ref)
 
-    pl.loop(0, 2)(finish)
+    pl.loop(0, 1)(finish)
+    complete(6, 2)
+    pl.loop(1, 2)(finish)
     ring_step(6)
     share(4)
     side(4).start()
-    complete(6, 2)
     pl.loop(2, PAIRS // GROUP)(finish)
     complete(5, 3)
 

time: 58.6 us -> 58.5 us (level)
  no operation moved by 1% of the time
where the time goes in v5:
time: 58.5 us; the launch traced here: 58.4 us
  Pallas kernels  56.5 us (97%)
  local copies, waits for them, and re-layouts  1.88 us (3%)
    pallas_call x1, Pallas kernels, per_device(): pl.pallas_call(kernel, out_shape=jax.ShapeDtypeStruct((C, 2048), BF16), i...  56.5 us
    unnamed x1, local copies, waits for them, and re-layouts  1.88 us

profile of v5, /device:TPU:1, one launch (start us, length us, event | category | flops | bytes accessed | tf_op | source)
XLA Modules:
  0.0 58.4 jit_solution(14950638381388138253)
XLA Ops:
  0.0 56.5 %mixer.1 = bf16[128,2048]{1,0:T(8,128)(2,1)} custom-call(bf16[128,2048]{1,0:T(8,128)(2,1)} %bitcast.9, bf16[128,2048]{1,0:T(8,128)(2,1)} %bitcast.10, bf16[128,2048]{1,0:T(8,128)(2,1)} %bitcast.11, bf16[128,128]{1,0:T(8,128)(2,1)} %bitcast.12, bf16[128,128]{1,0:T(8,128)(2,1)} %bitcast.13, bf16[128,2048]{1,0:T(8,128)(2,1)} %du_in.1, bf16[128,2048]{1,0:T(8,128)(2,1)} %ru_in.1, ...), custom_call_target="tpu_custom_call" | custom-call | tf_op jit(solution)/shard_map/mixer/pallas_call | solution.py:614
  56.5 1.9 %copy.12 = bf16[1,128,2048]{2,1,0:T(8,128)(2,1)} copy(bf16[1,128,2048]{2,1,0:T(8,128)(2,1)} %bitcast.8) | data formatting | bytes 1048576
